TPU v7x, 32 devices: a whole 2x2x4 slice. The times are simulated.
32 devices in a mesh: kv: 16 (over z, y, x), tp: 2 (over core).
Axes of the slice: x: 2, y: 2, z: 4, core: 2. Of those that a mesh axis runs over, the one named last changes fastest.
Arguments:
- stream: bfloat16 [32, 4096], P(None, 'kv'), may hold values from -32 to 32
- gain_in: bfloat16 [4096], P('kv'), may hold values from 0.099609375 to 1.8984375
- w_query: bfloat16 [4096, 2048], P('kv', 'tp'), may hold values from -0.09375 to 0.09375
- w_key: bfloat16 [4096, 2048], P('kv', 'tp'), may hold values from -0.09375 to 0.09375
- w_value: bfloat16 [4096, 2048], P('kv', 'tp'), may hold values from -0.09375 to 0.09375
- w_forget: bfloat16 [4096, 16], replicated, may hold values from -0.09375 to 0.09375
- keys_cache: bfloat16 [32, 16, 2048, 128], P(None, 'tp', 'kv'), may hold values from -136 to 136
- values_cache: bfloat16 [32, 16, 2048, 128], P(None, 'tp', 'kv'), may hold values from -6 to 6
- decay_cache: float32 [32, 16, 2048], P(None, 'tp', 'kv'), may hold values from -323 to 0
- lengths: int32 [32], replicated, may hold values from 1 to 2048, 26246 in all
- gain_att: bfloat16 [2048], P('tp'), may hold values from 0.099609375 to 1.8984375
- w_out: bfloat16 [2048, 4096], P('tp', 'kv'), may hold values from -0.125 to 0.125
- gain_mlp: bfloat16 [4096], P('kv'), may hold values from 0.099609375 to 1.8984375
- w_up: bfloat16 [4096, 16384], P('kv', 'tp'), may hold values from -0.09375 to 0.09375
- w_down: bfloat16 [16384, 4096], P('tp', 'kv'), may hold values from -0.046875 to 0.046875
Outputs:
- updated: bfloat16 [32, 4096], P(None, 'kv')
Inputs may be any that keep to these rules, and one draw needn't show every extreme that they name: `lengths`: one sequence has all 2048 positions live.
All inputs are finite; a program needn't handle non-finite values.
Results may differ from a plain program's by a relative error of at most 0.012.
The roundings to bfloat16 on the way count: a program that leaves them out, or rounds other values in their place, can miss the bound.
Values may be sent and summed in bfloat16 or wider, within the bound.
A program may use at most 64 MiB of HBM per device.

v0:
```python
import functools
import math

import jax
import jax.numpy as jnp
from jax import lax
from jax.experimental import pallas as pl
from jax.experimental.pallas import tpu as pltpu
from jax.sharding import PartitionSpec as P

f32 = jnp.float32
bf16 = jnp.bfloat16
LANES = 128

norm_eps = 1e-06
masked_score = -1e30


def merged_2(value, axis, join):
    pieces = jax.tree.map(lambda part: lax.all_gather(part, axis), value)
    head = jax.tree.map(lambda part: part[0], pieces)
    tail = jax.tree.map(lambda part: part[1:], pieces)
    so_far, _ = lax.scan(lambda so_far, share: (join(so_far, share), None), head, tail)
    return so_far


def fold_parts(left_part, right_part):
    peak_all = jnp.maximum(left_part[0], right_part[0])
    weight_one = jnp.exp(left_part[0] - peak_all)
    weight_two = jnp.exp(right_part[0] - peak_all)
    total_sum = left_part[1] * weight_one + right_part[1] * weight_two
    merged = left_part[2] * weight_one[..., None] + right_part[2] * weight_two[..., None]
    return (peak_all, total_sum, merged)


def per_device(
    stream,
    gain_in,
    w_query,
    w_key,
    w_value,
    w_forget,
    keys_cache,
    values_cache,
    decay_cache,
    lengths,
    gain_att,
    w_out,
    gain_mlp,
    w_up,
    w_down,
):
    kv_index = lax.axis_index("kv")
    tp_index = lax.axis_index("tp")
    kv_count = lax.axis_size("kv")
    seqs_here, cols_here = stream.shape
    heads_here = keys_cache.shape[1]
    pos_here = keys_cache.shape[2]
    head_dim = keys_cache.shape[3]
    width_all = cols_here * kv_count
    score_scale = 1.0 / math.sqrt(head_dim)
    stream_float = stream.astype(jnp.float32)
    scaled = (stream_float * gain_in.astype(jnp.float32)).astype(jnp.bfloat16)
    square_sum = jnp.sum(stream_float * stream_float, axis=1)
    forget_rows = lax.dynamic_slice(
        w_forget, (kv_index * cols_here, tp_index * heads_here), (cols_here, heads_here)
    )
    part_query = jnp.dot(scaled, w_query, preferred_element_type=jnp.float32)
    part_key = jnp.dot(scaled, w_key, preferred_element_type=jnp.float32)
    part_value = jnp.dot(scaled, w_value, preferred_element_type=jnp.float32)
    part_forget = jnp.dot(scaled, forget_rows, preferred_element_type=jnp.float32)
    part_query, part_key, part_value, part_forget, square_total = lax.psum(
        (part_query, part_key, part_value, part_forget, square_sum), "kv"
    )
    scale_in = lax.rsqrt(square_total / width_all + norm_eps)[:, None]
    queries = (part_query * scale_in).astype(jnp.bfloat16).reshape(seqs_here, heads_here, head_dim)
    key_new = (part_key * scale_in).astype(jnp.bfloat16).reshape(seqs_here, heads_here, head_dim)
    value_new = (
        (part_value * scale_in).astype(jnp.bfloat16).reshape(seqs_here, heads_here, head_dim)
    )
    forget = jax.nn.log_sigmoid(part_forget * scale_in)
    attention_logits = (
        jnp.einsum("shd,shpd->shp", queries, keys_cache, preferred_element_type=jnp.float32)
        * score_scale
    )
    attention_logits = attention_logits + forget[:, :, None] + decay_cache
    cache_positions = kv_index * pos_here + lax.iota(jnp.int32, pos_here)
    live_mask = (cache_positions[None, :] < lengths[:, None])[:, None, :]
    attention_logits = jnp.where(live_mask, attention_logits, masked_score)
    block_peak = jnp.max(attention_logits, axis=2)
    weights = jnp.where(live_mask, jnp.exp(attention_logits - block_peak[..., None]), 0.0)
    block_total = jnp.sum(weights, axis=2)
    block_out = jnp.einsum(
        "shp,shpd->shd",
        weights.astype(jnp.bfloat16),
        values_cache,
        preferred_element_type=jnp.float32,
    )
    peak_all, total_all, out_all = merged_2((block_peak, block_total, block_out), "kv", fold_parts)
    own_score = (
        jnp.sum(queries.astype(jnp.float32) * key_new.astype(jnp.float32), axis=2) * score_scale
    )
    top_score = jnp.maximum(peak_all, own_score)
    past_weight = jnp.exp(peak_all - top_score)
    own_weight = jnp.exp(own_score - top_score)
    numerator = (
        out_all * past_weight[..., None] + value_new.astype(jnp.float32) * own_weight[..., None]
    )
    denominator = total_all * past_weight + own_weight
    attended = (numerator / denominator[..., None]).reshape(seqs_here, heads_here * head_dim)
    attended_in = (attended * gain_att.astype(jnp.float32)).astype(jnp.bfloat16)
    part_out = jnp.dot(attended_in, w_out, preferred_element_type=jnp.float32)
    att_squares = jnp.sum(attended * attended, axis=1)
    part_out, att_total = lax.psum((part_out, att_squares), "tp")
    scale_att = lax.rsqrt(att_total / (attended.shape[1] * lax.axis_size("tp")) + norm_eps)[:, None]
    residual = (stream_float + scale_att * part_out).astype(jnp.bfloat16)
    residual_float = residual.astype(jnp.float32)
    mixer_in = (residual_float * gain_mlp.astype(jnp.float32)).astype(jnp.bfloat16)
    mixer_squares = jnp.sum(residual_float * residual_float, axis=1)
    part_up = jnp.dot(mixer_in, w_up, preferred_element_type=jnp.float32)
    pre_act, mixer_total = lax.psum((part_up, mixer_squares), "kv")
    scale_mixer = lax.rsqrt(mixer_total / width_all + norm_eps)[:, None]
    hidden = jnp.square(jax.nn.relu(pre_act * scale_mixer)).astype(jnp.bfloat16)
    part_down = jnp.dot(hidden, w_down, preferred_element_type=jnp.float32)
    mixer_out = lax.psum(part_down, "tp")
    return (residual_float + mixer_out).astype(jnp.bfloat16)


def thirds(value, group, wide):
    high = value.astype(bf16).astype(f32)
    rest = value - high
    mid = rest.astype(bf16).astype(f32)
    low = rest - mid
    third = group % 3 if wide else group
    picked = jnp.where(third == 0, high, jnp.where(third == 1, mid, low))
    return picked


def lanes_of(shape):
    return lax.broadcasted_iota(jnp.int32, shape, len(shape) - 1)


def layer_kernel(
    kv_n, heads_all, pos_here,
    lengths, stream, gain_in, gain_att, gain_mlp, decay,
    w_forget, w_query, w_key, w_value, keys, values, w_out, w_up, w_down,
    out,
    wf_v, wq_v, wk_v, wv_v, keys_v, values_v, wo_v, wu_v, wd_v,
    send1, recv1, q_all, q_float, o_float, s_float, send3, recv3, att_all,
    send5, recv5, send6, recv6, hid_all, send8, recv8,
    load_sem, cache_sem, ssem, rsem, pair_ssem, pair_rsem,
):
    me = lax.axis_index("kv")
    tp = lax.axis_index("tp")
    seqs, cols = stream.shape
    heads = decay.shape[1]
    dim = keys.shape[-1]
    rows = send1.shape[1] // 4
    groups = seqs // rows
    hidden_here = hid_all.shape[2]
    others = kv_n - 1
    chunks = cache_sem.shape[1]
    per_chunk = seqs // chunks
    score_scale = 1.0 / math.sqrt(dim)
    together = math.gcd(8, per_chunk)

    def load(src, dst, index):
        return pltpu.make_async_copy(src, dst, load_sem.at[index])

    start_row = pl.multiple_of(me * cols, cols)
    first_loads = [
        load(w_forget.at[:, pl.ds(start_row, cols)], wf_v, 0),
        load(w_query, wq_v, 1),
        load(w_key, wk_v, 2),
        load(w_value, wv_v, 3),
    ]
    for copy in first_loads:
        copy.start()

    def cache_copy(which, chunk):
        src, dst = ((keys, keys_v), (values, values_v))[which]
        part = pl.ds(chunk * per_chunk, per_chunk)
        return pltpu.make_async_copy(src.at[part], dst.at[part], cache_sem.at[which, chunk])

    late_loads = [load(w_out, wo_v, 4), load(w_up, wu_v, 5), load(w_down, wd_v, 6)]

    barrier = pltpu.get_barrier_semaphore()

    def greet(k, carry):
        pl.semaphore_signal(
            barrier, inc=1, device_id=(lax.rem(me + k, kv_n), tp),
            device_id_type=pl.DeviceIdType.MESH,
        )
        return carry

    lax.fori_loop(1, kv_n, greet, 0)
    pl.semaphore_signal(
        barrier, inc=1, device_id=(me, 1 - tp), device_id_type=pl.DeviceIdType.MESH
    )

    def partner(k):
        apart = kv_n - k
        bits = [1 << place for place in range(kv_n.bit_length() - 1)]
        return sum((((me // bit) + (apart // bit)) % 2) * bit for bit in bits)

    after = before = partner

    def remote(phase, k, src, dst):
        return pltpu.make_async_remote_copy(
            src_ref=src, dst_ref=dst,
            send_sem=ssem.at[phase, k - 1], recv_sem=rsem.at[phase, k - 1],
            device_id=(after(k), tp), device_id_type=pl.DeviceIdType.MESH,
        )

    def scatter(phase, k, send, recv):
        return remote(phase, k, send.at[after(k)], recv.at[k - 1])

    def spread(phase, k, held):
        return remote(phase, k, held.at[me], held.at[me])

    def landed(phase, k, held):
        return remote(phase, k, held.at[before(k)], held.at[before(k)])

    def each(body):
        lax.fori_loop(1, kv_n, lambda k, carry: (body(k), carry)[1], 0)

    def swap(index, src, dst):
        return pltpu.make_async_remote_copy(
            src_ref=src, dst_ref=dst, send_sem=pair_ssem.at[index],
            recv_sem=pair_rsem.at[index], device_id=(me, 1 - tp),
            device_id_type=pl.DeviceIdType.MESH,
        )

    x = stream[...].astype(f32)
    scaled = (x * gain_in[...].astype(f32).reshape(1, -1)).astype(bf16)
    squares = jnp.sum(x * x, axis=1, keepdims=True)
    for copy in first_loads:
        copy.wait()
    for chunk in range(chunks):
        cache_copy(0, chunk).start()
        cache_copy(1, chunk).start()
    for copy in late_loads:
        copy.start()
    lane = lanes_of((seqs, LANES))
    expand = lax.broadcasted_iota(jnp.int32, (heads_all, LANES), 0) == (
        lanes_of((heads_all, LANES)) % 32
    )
    wide_forget = lax.dot_general(
        wf_v[...], jnp.where(expand, 1.0, 0.0).astype(bf16), (((0,), (0,)), ((), ())),
        preferred_element_type=f32,
    ).astype(bf16)
    part_forget = jnp.dot(scaled, wide_forget, preferred_element_type=f32)
    stats = jnp.where(lane % 32 < heads_all, part_forget, squares)
    stats = thirds(stats, lane // 32, False)
    stats = jnp.where(lane < 96, stats, 0.0).astype(bf16)
    for place, weight in enumerate((wq_v, wk_v, wv_v)):
        part = jnp.dot(scaled, weight[...], preferred_element_type=f32).astype(bf16)
        for g in range(groups):
            for h in range(heads):
                send1[g * heads + h, place * rows:(place + 1) * rows, :] = part[
                    g * rows:(g + 1) * rows, h * dim:(h + 1) * dim
                ]
    for g in range(groups):
        for h in range(heads):
            send1[g * heads + h, 3 * rows:4 * rows, :] = stats[g * rows:(g + 1) * rows]
    pl.semaphore_wait(barrier, kv_n)
    each(lambda k: scatter(0, k, send1, recv1).start())

    def add1(k, total):
        scatter(0, k, send1, recv1).wait_recv()
        return total + recv1[k - 1].astype(f32)

    total = lax.fori_loop(1, kv_n, add1, send1[me].astype(f32))
    lane_r = lanes_of((rows, LANES))
    stat = total[3 * rows:]
    my_head = tp * heads + lax.rem(me, heads)
    forget_sum = jnp.sum(
        jnp.where(lane_r % 32 == my_head, stat, 0.0), axis=1, keepdims=True
    )
    square_sum = jnp.sum(
        jnp.where(lane_r % 32 == heads_all, stat, 0.0), axis=1, keepdims=True
    )
    width_all = cols * kv_n
    scale_in = lax.rsqrt(square_sum / width_all + norm_eps)
    query = (total[:rows] * scale_in).astype(bf16)
    key_new = (total[rows:2 * rows] * scale_in).astype(bf16).astype(f32)
    value_new = (total[2 * rows:3 * rows] * scale_in).astype(bf16).astype(f32)
    gate = forget_sum * scale_in
    forget = jnp.minimum(gate, 0.0) - jnp.log1p(jnp.exp(-jnp.abs(gate)))
    q_all[me] = query
    each(lambda k: spread(1, k, q_all).start())
    own_score = (
        jnp.sum(query.astype(f32) * key_new, axis=1, keepdims=True) * score_scale
    )
    each(lambda k: landed(1, k, q_all).wait_recv())

    q_float[...] = q_all[...].reshape(kv_n * rows, dim).astype(f32)
    head_row = lax.broadcasted_iota(jnp.int32, (heads, pos_here), 0)
    position = me * pos_here + lanes_of((heads, pos_here))
    lane_h = lanes_of((heads, LANES))

    def some_sequences(first_seq):
        batch = [first_seq + i for i in range(together)]
        places = [
            pl.ds((s // rows) * (heads * rows) + s % rows, heads, stride=rows) for s in batch
        ]
        q_parts = [q_float[mine, :].astype(bf16) for mine in places]
        everies = [
            lax.dot_general(
                q_s, keys_v[s].reshape(heads * pos_here, dim), (((1,), (1,)), ((), ())),
                preferred_element_type=f32,
            )
            for q_s, s in zip(q_parts, batch)
        ]
        spreads, stats = [], []
        for every, s in zip(everies, batch):
            score = every[:, :pos_here]
            for h in range(1, heads):
                score = jnp.where(
                    head_row == h, every[:, h * pos_here:(h + 1) * pos_here], score
                )
            score = score * score_scale + decay[s]
            live = position < lengths[s]
            score = jnp.where(live, score, masked_score)
            peak = jnp.max(score, axis=1, keepdims=True)
            probs = jnp.where(live, jnp.exp(score - peak), 0.0)
            block_total = jnp.sum(probs, axis=1, keepdims=True)
            spreads.append(jnp.concatenate(
                [jnp.where(head_row == h, probs, 0.0) for h in range(heads)], axis=1
            ).astype(bf16))
            stats.append(jnp.where(lane_h < 48, peak, block_total))
        outs = [
            jnp.dot(
                part, values_v[s].reshape(heads * pos_here, dim), preferred_element_type=f32
            )
            for part, s in zip(spreads, batch)
        ]
        for mine, out_s, stat_s in zip(places, outs, stats):
            o_float[mine, :] = out_s
            s_float[mine, :] = stat_s

    def one_chunk(chunk, carry):
        cache_copy(0, chunk).wait()
        cache_copy(1, chunk).wait()

        def inner(i, c):
            some_sequences(chunk * per_chunk + together * i)
            return c

        return lax.fori_loop(0, per_chunk // together, inner, carry)

    lax.fori_loop(0, chunks, one_chunk, 0)
    stats3 = s_float[...]
    stats3 = thirds(stats3, lanes_of(stats3.shape) // 16, True)
    send3[:, :rows, :] = o_float[...].astype(bf16).reshape(kv_n, rows, dim)
    send3[:, rows:, :] = stats3.astype(bf16).reshape(kv_n, rows, LANES)
    each(lambda k: scatter(2, k, send3, recv3).start())

    def opened(block):
        wide = block.astype(f32)
        stat = wide[rows:]
        is_third = lane_r % 16 == 0
        peak = jnp.sum(
            jnp.where(is_third & (lane_r < 48), stat, 0.0), axis=1, keepdims=True
        )
        total = jnp.sum(
            jnp.where(is_third & (lane_r >= 48) & (lane_r < 96), stat, 0.0),
            axis=1, keepdims=True,
        )
        return peak, total, wide[:rows]

    def fold3(k, so_far):
        scatter(2, k, send3, recv3).wait_recv()
        peak_a, total_a, out_a = so_far
        peak_b, total_b, out_b = opened(recv3[k - 1])
        peak = jnp.maximum(peak_a, peak_b)
        one, two = jnp.exp(peak_a - peak), jnp.exp(peak_b - peak)
        return peak, total_a * one + total_b * two, out_a * one + out_b * two

    peak_all, total_all, out_all = lax.fori_loop(1, kv_n, fold3, opened(send3[me]))
    peak_all = peak_all + forget
    top = jnp.maximum(peak_all, own_score)
    past_weight = jnp.exp(peak_all - top)
    own_weight = jnp.exp(own_score - top)
    att_all[me] = (out_all * past_weight + value_new * own_weight) / (
        total_all * past_weight + own_weight
    )
    each(lambda k: spread(3, k, att_all).start())
    each(lambda k: landed(3, k, att_all).wait_recv())
    attended = jnp.concatenate(
        [
            jnp.concatenate([att_all[g * heads + h] for g in range(groups)], axis=0)
            for h in range(heads)
        ],
        axis=1,
    )
    attended_in = (attended * gain_att[...].astype(f32).reshape(1, -1)).astype(bf16)
    late_loads[0].wait()
    part_out = jnp.dot(attended_in, wo_v[...], preferred_element_type=f32)
    att_squares = jnp.sum(attended * attended, axis=1, keepdims=True)
    send5[:, :cols] = part_out
    send5[:, cols:] = jnp.broadcast_to(att_squares, (seqs, LANES))
    swap5 = swap(0, send5, recv5)
    swap5.start()
    late_loads[1].wait()
    swap5.wait_recv()
    scale_att = lax.rsqrt(
        (att_squares + recv5[:, cols:cols + 1]) / (attended.shape[1] * 2) + norm_eps
    )
    residual = (
        stream[...].astype(f32) + scale_att * (part_out + recv5[:, :cols])
    ).astype(bf16).astype(f32)
    mixer_in = (residual * gain_mlp[...].astype(f32).reshape(1, -1)).astype(bf16)
    mixer_squares = jnp.sum(residual * residual, axis=1, keepdims=True)
    mixer_stats = thirds(jnp.broadcast_to(mixer_squares, (seqs, LANES)), lane, False)
    mixer_stats = jnp.where(lane < 3, mixer_stats, 0.0).astype(bf16)

    def up(owner):
        columns = pl.ds(pl.multiple_of(owner * hidden_here, LANES), hidden_here)
        send6[owner, :, :hidden_here] = jnp.dot(
            mixer_in, wu_v[:, columns], preferred_element_type=f32
        ).astype(bf16)
        send6[owner, :, hidden_here:] = mixer_stats

    def up_send(k):
        up(after(k))
        scatter(4, k, send6, recv6).start()

    each(up_send)
    up(me)

    def add6(k, total):
        scatter(4, k, send6, recv6).wait_recv()
        return total + recv6[k - 1].astype(f32)

    pre_act = lax.fori_loop(1, kv_n, add6, send6[me].astype(f32))
    mixer_total = jnp.sum(pre_act[:, hidden_here:], axis=1, keepdims=True)
    scale_mixer = lax.rsqrt(mixer_total / width_all + norm_eps)
    hidden = jnp.maximum(pre_act[:, :hidden_here] * scale_mixer, 0.0)
    hid_all[me] = (hidden * hidden).astype(bf16)
    each(lambda k: spread(5, k, hid_all).start())
    late_loads[2].wait()

    def down(owner):
        depth = pl.ds(pl.multiple_of(owner * hidden_here, LANES), hidden_here)
        return jnp.dot(hid_all[owner], wd_v[depth, :], preferred_element_type=f32)

    def add7(k, total):
        landed(5, k, hid_all).wait_recv()
        return total + down(before(k))

    part_down = lax.fori_loop(1, kv_n, add7, down(me))
    send8[...] = part_down
    swap8 = swap(1, send8, recv8)
    swap8.start()
    swap8.wait_recv()
    out[...] = (residual + (part_down + recv8[...])).astype(bf16)

    def drain(k):
        scatter(0, k, send1, recv1).wait_send()
        spread(1, k, q_all).wait_send()
        scatter(2, k, send3, recv3).wait_send()
        spread(3, k, att_all).wait_send()
        scatter(4, k, send6, recv6).wait_send()
        spread(5, k, hid_all).wait_send()

    each(drain)
    swap5.wait_send()
    swap8.wait_send()


def fits(kv_n, tp_n, seqs, cols, heads, heads_all, pos_here, dim, units):
    if tp_n != 2 or heads != 8 or (seqs * heads) % kv_n or units % kv_n or seqs % 32:
        return False
    rows = seqs * heads // kv_n
    return (
        rows % 16 == 0 and 4 % max(1, seqs // rows) == 0 and seqs % rows == 0
        and kv_n & (kv_n - 1) == 0 and cols % LANES == 0
        and pos_here == LANES and dim == LANES and heads_all <= 16
        and (units // kv_n) % LANES == 0
    )


def layer(
    stream, gain_in, w_query, w_key, w_value, w_forget, keys_cache, values_cache,
    decay_cache, lengths, gain_att, w_out, gain_mlp, w_up, w_down,
):
    kv_n, tp_n = lax.axis_size("kv"), lax.axis_size("tp")
    seqs, cols = stream.shape
    heads, pos_here, dim = keys_cache.shape[1:]
    heads_all = w_forget.shape[1]
    units = w_up.shape[1]
    if not fits(kv_n, tp_n, seqs, cols, heads, heads_all, pos_here, dim, units):
        return per_device(
            stream, gain_in, w_query, w_key, w_value, w_forget, keys_cache, values_cache,
            decay_cache, lengths, gain_att, w_out, gain_mlp, w_up, w_down,
        )
    rows = seqs * heads // kv_n
    hidden_here = units // kv_n
    others = kv_n - 1
    chunks = 4
    vmem = pl.BlockSpec(memory_space=pltpu.VMEM)
    anywhere = pl.BlockSpec(memory_space=pl.ANY)
    return pl.pallas_call(
        functools.partial(layer_kernel, kv_n, heads_all, pos_here),
        out_shape=jax.ShapeDtypeStruct((seqs, cols), bf16),
        in_specs=[pl.BlockSpec(memory_space=pltpu.SMEM)] + [vmem] * 5 + [anywhere] * 9,
        out_specs=vmem,
        scratch_shapes=[
            pltpu.VMEM((heads_all, cols), bf16),
            pltpu.VMEM(w_query.shape, bf16),
            pltpu.VMEM(w_key.shape, bf16),
            pltpu.VMEM(w_value.shape, bf16),
            pltpu.VMEM(keys_cache.shape, bf16),
            pltpu.VMEM(values_cache.shape, bf16),
            pltpu.VMEM(w_out.shape, bf16),
            pltpu.VMEM(w_up.shape, bf16),
            pltpu.VMEM(w_down.shape, bf16),
            pltpu.VMEM((kv_n, 4 * rows, dim), bf16),
            pltpu.VMEM((others, 4 * rows, dim), bf16),
            pltpu.VMEM((kv_n, rows, dim), bf16),
            pltpu.VMEM((kv_n * rows, dim), f32),
            pltpu.VMEM((kv_n * rows, dim), f32),
            pltpu.VMEM((kv_n * rows, LANES), f32),
            pltpu.VMEM((kv_n, 2 * rows, dim), bf16),
            pltpu.VMEM((others, 2 * rows, dim), bf16),
            pltpu.VMEM((kv_n, rows, dim), f32),
            pltpu.VMEM((seqs, cols + LANES), f32),
            pltpu.VMEM((seqs, cols + LANES), f32),
            pltpu.VMEM((kv_n, seqs, hidden_here + LANES), bf16),
            pltpu.VMEM((others, seqs, hidden_here + LANES), bf16),
            pltpu.VMEM((kv_n, seqs, hidden_here), bf16),
            pltpu.VMEM((seqs, cols), f32),
            pltpu.VMEM((seqs, cols), f32),
            pltpu.SemaphoreType.DMA((7,)),
            pltpu.SemaphoreType.DMA((2, chunks)),
            pltpu.SemaphoreType.DMA((6, others)),
            pltpu.SemaphoreType.DMA((6, others)),
            pltpu.SemaphoreType.DMA((2,)),
            pltpu.SemaphoreType.DMA((2,)),
        ],
        compiler_params=pltpu.CompilerParams(
            collective_id=0, has_side_effects=True, vmem_limit_bytes=60 * 1024 * 1024
        ),
    )(
        lengths, stream, gain_in, gain_att,
        gain_mlp, decay_cache,
        w_forget.T, w_query, w_key, w_value, keys_cache, values_cache, w_out, w_up, w_down,
    )


def solution(mesh):
    in_specs = (
        P(None, "kv"),
        P("kv"),
        P("kv", "tp"),
        P("kv", "tp"),
        P("kv", "tp"),
        P(),
        P(None, "tp", "kv", None),
        P(None, "tp", "kv", None),
        P(None, "tp", "kv"),
        P(),
        P("tp"),
        P("tp", "kv"),
        P("kv"),
        P("kv", "tp"),
        P("tp", "kv"),
    )
    out_specs = P(None, "kv")
    return jax.shard_map(
        layer, mesh=mesh, in_specs=in_specs, out_specs=out_specs, check_vma=False
    )
```

profile of v0, /device:TPU:0, one launch (start us, length us, event | category | flops | bytes accessed | tf_op | source)
XLA Modules:
  0.0 68.5 jit_solution(14243189732407616436)
XLA Ops:
  0.0 67.2 %shard_map.145 = bf16[32,256]{1,0:T(8,128)(2,1)} custom-call(s32[32]{0:T(128)} %lengths.1, bf16[32,256]{1,0:T(8,128)(2,1)} %stream.1, bf16[256]{0:T(256)(128)(2,1)} %gain_in.1, bf16[1024]{0:T(1024)(128)(2,1)} %gain_att.1, bf16[256]{0:T(256)(128)(2,1)} %gain_mlp.1, f32[32,8,128]{2,1,0:T(8,128)} %decay.1, bf16[16,4096]{1,0:T(8,128)(2,1)} %bitcast.1, ...), custom_call_target="tpu_custom_call" | custom-call | tf_op jit(solution)/shard_map/pallas_call | solution.py:504
  67.2 1.3 %copy.17 = bf16[32,256]{1,0:T(8,128)(2,1)} copy(bf16[32,256]{1,0:T(8,128)(2,1)} %shard_map.145) | data formatting | bytes 32768
where the time goes:
time: 68.8 us; the launch traced here: 68.5 us
  Pallas kernels  67.2 us (98%)
  local copies, waits for them, and re-layouts  1.32 us (2%)
    pallas_call x1, Pallas kernels, layer(): pl.pallas_call(functools.partial(layer_kernel, kv_n, heads_all, pos_here)...  67.2 us

commit v1 on v0

v1 whole, which is shorter than its diff:
```python
import functools
import math

import jax
import jax.numpy as jnp
from jax import lax
from jax.experimental import pallas as pl
from jax.experimental.pallas import tpu as pltpu
from jax.sharding import PartitionSpec as P

f32 = jnp.float32
bf16 = jnp.bfloat16
LANES = 128
PLANE = 4

norm_eps = 1e-06
masked_score = -1e30


def merged_2(value, axis, join):
    pieces = jax.tree.map(lambda part: lax.all_gather(part, axis), value)
    head = jax.tree.map(lambda part: part[0], pieces)
    tail = jax.tree.map(lambda part: part[1:], pieces)
    so_far, _ = lax.scan(lambda so_far, share: (join(so_far, share), None), head, tail)
    return so_far


def fold_parts(left_part, right_part):
    peak_all = jnp.maximum(left_part[0], right_part[0])
    weight_one = jnp.exp(left_part[0] - peak_all)
    weight_two = jnp.exp(right_part[0] - peak_all)
    total_sum = left_part[1] * weight_one + right_part[1] * weight_two
    merged = left_part[2] * weight_one[..., None] + right_part[2] * weight_two[..., None]
    return (peak_all, total_sum, merged)


def per_device(
    stream,
    gain_in,
    w_query,
    w_key,
    w_value,
    w_forget,
    keys_cache,
    values_cache,
    decay_cache,
    lengths,
    gain_att,
    w_out,
    gain_mlp,
    w_up,
    w_down,
):
    kv_index = lax.axis_index("kv")
    tp_index = lax.axis_index("tp")
    kv_count = lax.axis_size("kv")
    seqs_here, cols_here = stream.shape
    heads_here = keys_cache.shape[1]
    pos_here = keys_cache.shape[2]
    head_dim = keys_cache.shape[3]
    width_all = cols_here * kv_count
    score_scale = 1.0 / math.sqrt(head_dim)
    stream_float = stream.astype(jnp.float32)
    scaled = (stream_float * gain_in.astype(jnp.float32)).astype(jnp.bfloat16)
    square_sum = jnp.sum(stream_float * stream_float, axis=1)
    forget_rows = lax.dynamic_slice(
        w_forget, (kv_index * cols_here, tp_index * heads_here), (cols_here, heads_here)
    )
    part_query = jnp.dot(scaled, w_query, preferred_element_type=jnp.float32)
    part_key = jnp.dot(scaled, w_key, preferred_element_type=jnp.float32)
    part_value = jnp.dot(scaled, w_value, preferred_element_type=jnp.float32)
    part_forget = jnp.dot(scaled, forget_rows, preferred_element_type=jnp.float32)
    part_query, part_key, part_value, part_forget, square_total = lax.psum(
        (part_query, part_key, part_value, part_forget, square_sum), "kv"
    )
    scale_in = lax.rsqrt(square_total / width_all + norm_eps)[:, None]
    queries = (part_query * scale_in).astype(jnp.bfloat16).reshape(seqs_here, heads_here, head_dim)
    key_new = (part_key * scale_in).astype(jnp.bfloat16).reshape(seqs_here, heads_here, head_dim)
    value_new = (
        (part_value * scale_in).astype(jnp.bfloat16).reshape(seqs_here, heads_here, head_dim)
    )
    forget = jax.nn.log_sigmoid(part_forget * scale_in)
    attention_logits = (
        jnp.einsum("shd,shpd->shp", queries, keys_cache, preferred_element_type=jnp.float32)
        * score_scale
    )
    attention_logits = attention_logits + forget[:, :, None] + decay_cache
    cache_positions = kv_index * pos_here + lax.iota(jnp.int32, pos_here)
    live_mask = (cache_positions[None, :] < lengths[:, None])[:, None, :]
    attention_logits = jnp.where(live_mask, attention_logits, masked_score)
    block_peak = jnp.max(attention_logits, axis=2)
    weights = jnp.where(live_mask, jnp.exp(attention_logits - block_peak[..., None]), 0.0)
    block_total = jnp.sum(weights, axis=2)
    block_out = jnp.einsum(
        "shp,shpd->shd",
        weights.astype(jnp.bfloat16),
        values_cache,
        preferred_element_type=jnp.float32,
    )
    peak_all, total_all, out_all = merged_2((block_peak, block_total, block_out), "kv", fold_parts)
    own_score = (
        jnp.sum(queries.astype(jnp.float32) * key_new.astype(jnp.float32), axis=2) * score_scale
    )
    top_score = jnp.maximum(peak_all, own_score)
    past_weight = jnp.exp(peak_all - top_score)
    own_weight = jnp.exp(own_score - top_score)
    numerator = (
        out_all * past_weight[..., None] + value_new.astype(jnp.float32) * own_weight[..., None]
    )
    denominator = total_all * past_weight + own_weight
    attended = (numerator / denominator[..., None]).reshape(seqs_here, heads_here * head_dim)
    attended_in = (attended * gain_att.astype(jnp.float32)).astype(jnp.bfloat16)
    part_out = jnp.dot(attended_in, w_out, preferred_element_type=jnp.float32)
    att_squares = jnp.sum(attended * attended, axis=1)
    part_out, att_total = lax.psum((part_out, att_squares), "tp")
    scale_att = lax.rsqrt(att_total / (attended.shape[1] * lax.axis_size("tp")) + norm_eps)[:, None]
    residual = (stream_float + scale_att * part_out).astype(jnp.bfloat16)
    residual_float = residual.astype(jnp.float32)
    mixer_in = (residual_float * gain_mlp.astype(jnp.float32)).astype(jnp.bfloat16)
    mixer_squares = jnp.sum(residual_float * residual_float, axis=1)
    part_up = jnp.dot(mixer_in, w_up, preferred_element_type=jnp.float32)
    pre_act, mixer_total = lax.psum((part_up, mixer_squares), "kv")
    scale_mixer = lax.rsqrt(mixer_total / width_all + norm_eps)[:, None]
    hidden = jnp.square(jax.nn.relu(pre_act * scale_mixer)).astype(jnp.bfloat16)
    part_down = jnp.dot(hidden, w_down, preferred_element_type=jnp.float32)
    mixer_out = lax.psum(part_down, "tp")
    return (residual_float + mixer_out).astype(jnp.bfloat16)


def lanes_of(shape):
    return lax.broadcasted_iota(jnp.int32, shape, 1)


def rows_of(shape):
    return lax.broadcasted_iota(jnp.int32, shape, 0)


def to_column(row, count, *starts):
    shape = (count, LANES)
    apart = lanes_of(shape) - rows_of(shape)
    hit = functools.reduce(jnp.logical_or, [apart == start for start in starts])
    return jnp.sum(
        jnp.where(hit, jnp.broadcast_to(row, shape), 0.0), axis=1, keepdims=True
    )


def to_row(column, start):
    shape = (column.shape[0], LANES)
    hit = lanes_of(shape) - rows_of(shape) == start
    return jnp.sum(
        jnp.where(hit, jnp.broadcast_to(column, shape), 0.0), axis=0, keepdims=True
    )


Q, STAT, KV, Q_ALL, OUT, PEAK, ATT, SQUARE, MIX, UP, RELAY, HID, HID_RELAY, PAIR = range(14)


def layer_kernel(
    kv_n,
    lengths, stream, gain_in, gain_att, gain_mlp, decay,
    w_forget, w_query, w_key, w_value, keys, values, w_out, w_up, w_down,
    out,
    len_s, x_v, gi_v, ga_v, gm_v, decay_v,
    wf_v, wq_v, wk_v, wv_v, keys_v, values_v, wo_v, wu_v, wd_v,
    gain_far, q_send, q_recv, st_send, st_recv, kv_send, kv_recv,
    q_own, q_all, q_float, o_float, o_send, o_recv, pk_send, pk_recv,
    att_own, att_all, sq_own, sq_all, send5, recv5,
    mix_own, mix_all, up_send, relay_recv, relay_send, up_recv,
    hid_relay, hid_all, send8, recv8,
    load_sem, cache_sem, ssem, rsem,
):
    me = lax.axis_index("kv")
    tp = lax.axis_index("tp")
    far = 1 - tp
    seqs, cols = x_v.shape
    heads = decay_v.shape[1]
    pos_here = decay_v.shape[2]
    dim = keys_v.shape[-1]
    rows = q_own.shape[0]
    groups = seqs // rows
    hidden_here = hid_all.shape[2]
    chunks = cache_sem.shape[1]
    per_chunk = seqs // chunks
    width_all = cols * kv_n
    score_scale = 1.0 / math.sqrt(dim)
    together = math.gcd(8, per_chunk)

    level, spot = me // PLANE, me % PLANE
    levels = (level, level + 1 - 2 * (level % 2), (level + 2) % 4, 3 - level)
    side, along = spot // 2, spot % 2
    spots = (
        spot, side * 2 + 1 - along, (1 - side) * 2 + along, (1 - side) * 2 + 1 - along
    )
    peers = [levels[k // PLANE] * PLANE + spots[k % PLANE] for k in range(kv_n)]
    far_first = (15, 14, 13, 11, 12, 10, 9, 7, 8, 6, 5, 3, 4, 2, 1, 0)
    plane_order = (3, 1, 2, 0)
    my_group, my_head = me // heads, me % heads

    barrier = pltpu.get_barrier_semaphore()
    for k in far_first:
        pl.semaphore_signal(
            barrier, inc=1, device_id=(peers[k], far), device_id_type=pl.DeviceIdType.MESH
        )

    def load(src, dst, index):
        return pltpu.make_async_copy(src, dst, load_sem.at[index])

    start_row = pl.multiple_of(me * cols, cols)
    first_head = pl.multiple_of(tp * heads, heads)
    first_loads = [
        load(stream, x_v, 0),
        load(gain_in, gi_v, 1),
        load(w_query, wq_v, 2),
        load(w_forget.at[pl.ds(first_head, heads), pl.ds(start_row, cols)], wf_v, 3),
        load(w_key, wk_v, 4),
        load(w_value, wv_v, 5),
    ]
    small_loads = [
        load(gain_att, ga_v, 6), load(decay, decay_v, 7), load(lengths, len_s, 8),
        load(gain_mlp, gm_v, 9),
    ]
    late_loads = [load(w_out, wo_v, 10), load(w_up, wu_v, 11), load(w_down, wd_v, 12)]
    for copy in first_loads:
        copy.start()
    for copy in small_loads:
        copy.start()

    def cache_copy(which, chunk):
        src, dst = ((keys, keys_v), (values, values_v))[which]
        part = pl.ds(chunk * per_chunk, per_chunk)
        return pltpu.make_async_copy(src.at[part], dst.at[part], cache_sem.at[which, chunk])

    def remote(phase, slot, src, dst, device, core):
        return pltpu.make_async_remote_copy(
            src_ref=src, dst_ref=dst,
            send_sem=ssem.at[phase, slot], recv_sem=rsem.at[phase, slot],
            device_id=(device, core), device_id_type=pl.DeviceIdType.MESH,
        )

    started = []

    def go(copy):
        copy.start()
        started.append(copy)

    def drain():
        for copy in started:
            copy.wait_send()
        started.clear()

    def scatter(phase, send, recv, k):
        return remote(phase, k, send.at[peers[k]], recv.at[k], peers[k], far)

    def row_to(phase, src, recv, k):
        return remote(phase, k, src, recv.at[pl.ds(k, 1)], peers[k], far)

    def spread(phase, own, held, k):
        return remote(phase, k, own, held.at[me], peers[k], far)

    def landed(phase, own, held, k):
        return remote(phase, k, own, held.at[peers[k]], peers[k], far)

    for copy in first_loads[:4]:
        copy.wait()
    x = x_v[...].astype(f32)
    scaled = (x * gi_v[...].astype(f32).reshape(1, -1)).astype(bf16)

    def by_owner(dst, part, place):
        for g in range(groups):
            for h in range(heads):
                dst[g * heads + h, place * rows:(place + 1) * rows, :] = part[
                    g * rows:(g + 1) * rows, h * dim:(h + 1) * dim
                ]

    by_owner(q_send, jnp.dot(scaled, wq_v[...], preferred_element_type=f32).astype(bf16), 0)
    squares = x * x
    high = squares.astype(bf16)
    low = (squares - high.astype(f32)).astype(bf16)
    blank = jnp.zeros((32, cols), bf16)
    last = (((1,), (1,)), ((), ()))
    st_send[...] = lax.dot_general(
        jnp.ones((heads, cols), bf16), jnp.concatenate([high, blank, low, blank], axis=0),
        last, preferred_element_type=f32,
    ) + lax.dot_general(
        wf_v[...], jnp.concatenate([blank, scaled, blank, blank], axis=0),
        last, preferred_element_type=f32,
    )
    for copy in first_loads[4:]:
        copy.wait()
    for copy in small_loads:
        copy.wait()
    for chunk in range(chunks):
        cache_copy(0, chunk).start()
        cache_copy(1, chunk).start()
    for copy in late_loads:
        copy.start()
    pl.semaphore_wait(barrier, kv_n)
    for k in far_first:
        go(scatter(Q, q_send, q_recv, k))
        go(row_to(STAT, st_send.at[pl.ds(peers[k] % heads, 1)], st_recv, k))
    gain_swap = remote(PAIR, 0, ga_v, gain_far, me, far)
    go(gain_swap)
    for place, weight in enumerate((wk_v, wv_v)):
        by_owner(
            kv_send, jnp.dot(scaled, weight[...], preferred_element_type=f32).astype(bf16), place
        )
    for k in far_first:
        go(scatter(KV, kv_send, kv_recv, k))
    total = jnp.zeros((rows, dim), f32)
    for k in range(kv_n):
        row_to(STAT, st_send.at[pl.ds(0, 1)], st_recv, k).wait_recv()
        scatter(Q, q_send, q_recv, k).wait_recv()
        total = total + q_recv[k].astype(f32)
    stat_row = jnp.sum(st_recv[...], axis=0, keepdims=True)
    first_lane = my_group * rows
    scale_in = lax.rsqrt(
        to_column(stat_row, rows, first_lane, first_lane + 64) / width_all + norm_eps
    )
    query = (total * scale_in).astype(bf16)
    q_own[...] = query
    for k in far_first:
        go(spread(Q_ALL, q_own, q_all, k))
    gate = to_column(stat_row, rows, first_lane + 32) * scale_in
    forget = jnp.minimum(gate, 0.0) - jnp.log1p(jnp.exp(-jnp.abs(gate)))

    for k in range(kv_n):
        landed(Q_ALL, q_own, q_all, k).wait_recv()
    q_float[...] = q_all[...].reshape(kv_n * rows, dim).astype(f32)
    head_row = rows_of((heads, pos_here))
    position = me * pos_here + lanes_of((heads, pos_here))
    lane_h = lanes_of((heads, LANES))

    def some_sequences(first_seq, marks):
        batch = [first_seq + i for i in range(together)]
        places = [
            pl.ds((s // rows) * (heads * rows) + s % rows, heads, stride=rows) for s in batch
        ]
        q_parts = [q_float[mine, :].astype(bf16) for mine in places]
        everies = [
            lax.dot_general(
                q_s, keys_v[s].reshape(heads * pos_here, dim), last,
                preferred_element_type=f32,
            )
            for q_s, s in zip(q_parts, batch)
        ]
        spreads = []
        for every, s in zip(everies, batch):
            score = every[:, :pos_here]
            for h in range(1, heads):
                score = jnp.where(
                    head_row == h, every[:, h * pos_here:(h + 1) * pos_here], score
                )
            score = score * score_scale + decay_v[s]
            live = position < len_s[s]
            score = jnp.where(live, score, masked_score)
            peak = jnp.max(score, axis=1, keepdims=True)
            probs = jnp.where(live, jnp.exp(score - peak), 0.0)
            block_total = jnp.sum(probs, axis=1, keepdims=True)
            spreads.append(jnp.concatenate(
                [jnp.where(head_row == h, probs, 0.0) for h in range(heads)], axis=1
            ).astype(bf16))
            marks = jnp.where(lane_h == s % rows, peak, marks)
            marks = jnp.where(lane_h == s % rows + rows, block_total, marks)
        outs = [
            jnp.dot(
                part, values_v[s].reshape(heads * pos_here, dim), preferred_element_type=f32
            )
            for part, s in zip(spreads, batch)
        ]
        for mine, out_s in zip(places, outs):
            o_float[mine, :] = out_s
        return marks

    def one_chunk(chunk, marks):
        cache_copy(0, chunk).wait()
        cache_copy(1, chunk).wait()

        def inner(i, c):
            return some_sequences(chunk * per_chunk + together * i, c)

        return lax.fori_loop(0, per_chunk // together, inner, marks)

    group_chunks = chunks // groups
    for g in range(groups):
        marks = lax.fori_loop(
            g * group_chunks, (g + 1) * group_chunks, one_chunk, jnp.zeros((heads, LANES), f32)
        )
        pk_send[g * heads:(g + 1) * heads, :] = marks
    o_send[...] = o_float[...].astype(bf16).reshape(kv_n, rows, dim)
    for k in far_first:
        go(scatter(OUT, o_send, o_recv, k))
        go(row_to(PEAK, pk_send.at[pl.ds(peers[k], 1)], pk_recv, k))

    keys_total = jnp.zeros((2 * rows, dim), f32)
    for k in range(kv_n):
        scatter(KV, kv_send, kv_recv, k).wait_recv()
        keys_total = keys_total + kv_recv[k].astype(f32)
    key_new = (keys_total[:rows] * scale_in).astype(bf16).astype(f32)
    value_new = (keys_total[rows:] * scale_in).astype(bf16).astype(f32)
    own_score = jnp.sum(query.astype(f32) * key_new, axis=1, keepdims=True) * score_scale
    gain_swap.wait_recv()
    gain_here = gain_far[...].astype(f32).reshape(1, -1)
    gain_head = gain_here[:, :dim]
    for h in range(1, heads):
        gain_head = jnp.where(my_head == h, gain_here[:, h * dim:(h + 1) * dim], gain_head)

    for k in range(kv_n):
        row_to(PEAK, pk_send.at[pl.ds(0, 1)], pk_recv, k).wait_recv()
    peaks = pk_recv[...]
    top_row = jnp.max(peaks, axis=0, keepdims=True)
    shares = jnp.exp(peaks - top_row)
    total_row = jnp.sum(shares * pltpu.roll(peaks, LANES - rows, 1), axis=0, keepdims=True)
    peak_all = to_column(top_row, rows, 0) + forget
    total_all = to_column(total_row, rows, 0)
    share_columns = [to_column(shares[k:k + 1], rows, 0) for k in range(kv_n)]
    top = jnp.maximum(peak_all, own_score)
    past_weight = jnp.exp(peak_all - top)
    own_weight = jnp.exp(own_score - top)
    out_all = jnp.zeros((rows, dim), f32)
    for k in range(kv_n):
        scatter(OUT, o_send, o_recv, k).wait_recv()
        out_all = out_all + share_columns[k] * o_recv[k].astype(f32)
    attended_one = (out_all * past_weight + value_new * own_weight) / (
        total_all * past_weight + own_weight
    )
    att_own[...] = (attended_one * gain_head).astype(bf16)
    squares_one = jnp.sum(attended_one * attended_one, axis=1, keepdims=True)
    sq_own[...] = jnp.broadcast_to(to_row(squares_one, first_lane), sq_own.shape)
    for k in far_first:
        go(spread(ATT, att_own, att_all, k))
        go(row_to(SQUARE, sq_own.at[pl.ds(0, 1)], sq_all, k))

    for copy in late_loads:
        copy.wait()
    drain_before = list(started[:-2 * kv_n])
    for copy in drain_before:
        copy.wait_send()
    del started[:len(drain_before)]
    for k in range(kv_n):
        landed(ATT, att_own, att_all, k).wait_recv()
        row_to(SQUARE, sq_own.at[pl.ds(0, 1)], sq_all, k).wait_recv()
    attended_in = jnp.concatenate(
        [
            jnp.concatenate([att_all[g * heads + h] for g in range(groups)], axis=0)
            for h in range(heads)
        ],
        axis=1,
    )
    part_out = jnp.dot(attended_in, wo_v[...], preferred_element_type=f32)
    att_squares = to_column(jnp.sum(sq_all[...], axis=0, keepdims=True), seqs, 0)
    send5[:, :cols] = part_out
    send5[:, cols:] = jnp.broadcast_to(att_squares, (seqs, LANES))
    swap5 = remote(PAIR, 1, send5, recv5, me, far)
    go(swap5)
    swap5.wait_recv()
    width_att = attended_in.shape[1] * 2
    scale_att = lax.rsqrt((att_squares + recv5[:, cols:cols + 1]) / width_att + norm_eps)
    residual = (
        x_v[...].astype(f32) + scale_att * (part_out + recv5[:, :cols])
    ).astype(bf16).astype(f32)
    mixer_in = (residual * gm_v[...].astype(f32).reshape(1, -1)).astype(bf16)
    mixer_squares = jnp.sum(residual * residual, axis=1, keepdims=True)

    def up(owner):
        columns = pl.ds(pl.multiple_of(owner * hidden_here, LANES), hidden_here)
        return jnp.dot(mixer_in, wu_v[:, columns], preferred_element_type=f32)

    def to_relay(k):
        return remote(
            UP, k, up_send.at[k], relay_recv.at[k - 2 * PLANE], peers[k % PLANE], far
        )

    def from_relay(apart):
        index = apart - 2
        return remote(
            RELAY, index, relay_send.at[index], up_recv.at[index], peers[apart * PLANE], far
        )

    def straight(k):
        return remote(UP, k, up_send.at[k], up_recv.at[k + 1], peers[k], tp)

    for apart in (3, 2):
        for p in plane_order:
            k = apart * PLANE + p
            up_send[k] = up(peers[k]).astype(bf16)
            go(to_relay(k))
    mix_own[...] = jnp.broadcast_to(to_row(mixer_squares, 0), mix_own.shape)
    for k in far_first:
        go(row_to(MIX, mix_own.at[pl.ds(0, 1)], mix_all, k))
    for apart in (1, 0):
        for p in plane_order:
            k = apart * PLANE + p
            if k:
                up_send[k] = up(peers[k]).astype(bf16)
                go(straight(k))
    pre_act = up(me)
    for apart in (3, 2):
        relayed = None
        for p in (0, 1, 2, 3):
            k = apart * PLANE + p
            to_relay(k).wait_recv()
            block = relay_recv[k - 2 * PLANE].astype(f32)
            relayed = block if relayed is None else relayed + block
        relay_send[apart - 2] = relayed.astype(bf16)
        go(from_relay(apart))
    for k in range(kv_n):
        row_to(MIX, mix_own.at[pl.ds(0, 1)], mix_all, k).wait_recv()
    mixer_total = to_column(jnp.sum(mix_all[...], axis=0, keepdims=True), seqs, 0)
    scale_mixer = lax.rsqrt(mixer_total / width_all + norm_eps)
    for k in range(1, 2 * PLANE):
        straight(k).wait_recv()
        pre_act = pre_act + up_recv[k + 1].astype(f32)
    for apart in (2, 3):
        from_relay(apart).wait_recv()
        pre_act = pre_act + up_recv[apart - 2].astype(f32)
    hidden = jnp.maximum(pre_act * scale_mixer, 0.0)
    hid_all[me] = (hidden * hidden).astype(bf16)

    def to_level(apart):
        return remote(
            HID_RELAY, apart - 2, hid_all.at[me], hid_relay.at[apart - 2],
            peers[apart * PLANE], far,
        )

    def onward(apart, p):
        return remote(
            HID, apart * PLANE + p, hid_relay.at[apart - 2],
            hid_all.at[peers[apart * PLANE]], peers[p], far,
        )

    def arrived(k):
        return remote(HID, k, hid_all.at[me], hid_all.at[peers[k]], peers[k], tp)

    for apart in (3, 2):
        go(to_level(apart))
    for apart in (0, 1):
        for p in plane_order:
            k = apart * PLANE + p
            if k:
                go(remote(HID, k, hid_all.at[me], hid_all.at[me], peers[k], tp))

    def down(owner):
        depth = pl.ds(pl.multiple_of(owner * hidden_here, LANES), hidden_here)
        return jnp.dot(hid_all[owner], wd_v[depth, :], preferred_element_type=f32)

    part_down = down(me)
    for apart in (2, 3):
        to_level(apart).wait_recv()
        for p in plane_order:
            go(onward(apart, p))
    for k in range(1, kv_n):
        arrived(k).wait_recv()
        part_down = part_down + down(peers[k])
    send8[...] = part_down
    swap8 = remote(PAIR, 2, send8, recv8, me, far)
    go(swap8)
    drain_before = list(started[:-1])
    for copy in drain_before:
        copy.wait_send()
    swap8.wait_recv()
    out[...] = (residual + (part_down + recv8[...])).astype(bf16)
    swap8.wait_send()


def fits(kv_n, tp_n, seqs, cols, heads, heads_all, pos_here, dim, units):
    if tp_n != 2 or kv_n != PLANE * PLANE or heads != 8 or seqs != 32:
        return False
    return (
        cols % LANES == 0 and pos_here == LANES and dim == LANES
        and heads_all == 2 * heads and units % (kv_n * LANES) == 0
    )


def layer(
    stream, gain_in, w_query, w_key, w_value, w_forget, keys_cache, values_cache,
    decay_cache, lengths, gain_att, w_out, gain_mlp, w_up, w_down,
):
    kv_n, tp_n = lax.axis_size("kv"), lax.axis_size("tp")
    seqs, cols = stream.shape
    heads, pos_here, dim = keys_cache.shape[1:]
    heads_all = w_forget.shape[1]
    units = w_up.shape[1]
    if not fits(kv_n, tp_n, seqs, cols, heads, heads_all, pos_here, dim, units):
        return per_device(
            stream, gain_in, w_query, w_key, w_value, w_forget, keys_cache, values_cache,
            decay_cache, lengths, gain_att, w_out, gain_mlp, w_up, w_down,
        )
    rows = seqs * heads // kv_n
    hidden_here = units // kv_n
    chunks = 4
    anywhere = pl.BlockSpec(memory_space=pl.ANY)

    def held(*shape, kind=bf16):
        return pltpu.VMEM(shape, kind)

    return pl.pallas_call(
        functools.partial(layer_kernel, kv_n),
        out_shape=jax.ShapeDtypeStruct((seqs, cols), bf16),
        in_specs=[anywhere] * 15,
        out_specs=pl.BlockSpec(memory_space=pltpu.VMEM),
        scratch_shapes=[
            pltpu.SMEM((seqs,), jnp.int32),
            held(seqs, cols),
            held(cols),
            held(*gain_att.shape),
            held(cols),
            held(*decay_cache.shape, kind=f32),
            held(heads, cols),
            held(*w_query.shape),
            held(*w_key.shape),
            held(*w_value.shape),
            held(*keys_cache.shape),
            held(*values_cache.shape),
            held(*w_out.shape),
            held(*w_up.shape),
            held(*w_down.shape),
            held(*gain_att.shape),
            held(kv_n, rows, dim),
            held(kv_n, rows, dim),
            held(heads, LANES, kind=f32),
            held(kv_n, LANES, kind=f32),
            held(kv_n, 2 * rows, dim),
            held(kv_n, 2 * rows, dim),
            held(rows, dim),
            held(kv_n, rows, dim),
            held(kv_n * rows, dim, kind=f32),
            held(kv_n * rows, dim, kind=f32),
            held(kv_n, rows, dim),
            held(kv_n, rows, dim),
            held(kv_n, LANES, kind=f32),
            held(kv_n, LANES, kind=f32),
            held(rows, dim),
            held(kv_n, rows, dim),
            held(8, LANES, kind=f32),
            held(kv_n, LANES, kind=f32),
            held(seqs, cols + LANES, kind=f32),
            held(seqs, cols + LANES, kind=f32),
            held(8, LANES, kind=f32),
            held(kv_n, LANES, kind=f32),
            held(kv_n, seqs, hidden_here),
            held(2 * PLANE, seqs, hidden_here),
            held(2, seqs, hidden_here),
            held(2 * PLANE + 1, seqs, hidden_here),
            held(2, seqs, hidden_here),
            held(kv_n, seqs, hidden_here),
            held(seqs, cols, kind=f32),
            held(seqs, cols, kind=f32),
            pltpu.SemaphoreType.DMA((13,)),
            pltpu.SemaphoreType.DMA((2, chunks)),
            pltpu.SemaphoreType.DMA((14, kv_n)),
            pltpu.SemaphoreType.DMA((14, kv_n)),
        ],
        compiler_params=pltpu.CompilerParams(
            collective_id=0, has_side_effects=True, vmem_limit_bytes=60 * 1024 * 1024
        ),
    )(
        lengths, stream, gain_in, gain_att,
        gain_mlp, decay_cache,
        w_forget.T, w_query, w_key, w_value, keys_cache, values_cache, w_out, w_up, w_down,
    )


def solution(mesh):
    in_specs = (
        P(None, "kv"),
        P("kv"),
        P("kv", "tp"),
        P("kv", "tp"),
        P("kv", "tp"),
        P(),
        P(None, "tp", "kv", None),
        P(None, "tp", "kv", None),
        P(None, "tp", "kv"),
        P(),
        P("tp"),
        P("tp", "kv"),
        P("kv"),
        P("kv", "tp"),
        P("tp", "kv"),
    )
    out_specs = P(None, "kv")
    return jax.shard_map(
        layer, mesh=mesh, in_specs=in_specs, out_specs=out_specs, check_vma=False
    )
```

time: 68.8 us -> 55.2 us (0.80)
  Pallas kernels: 67.2 us -> 53.6 us
    pallas_call x1, Pallas kernels: 67.2 us -> 53.6 us  [layer(): pl.pallas_call(functools.partial(layer_kernel, kv_n), out_shape=jax.Shape...]
where the time goes in v1:
time: 55.2 us; the launch traced here: 54.9 us
  Pallas kernels  53.6 us (97%)
  local copies, waits for them, and re-layouts  1.32 us (2%)
    pallas_call x1, Pallas kernels, layer(): pl.pallas_call(functools.partial(layer_kernel, kv_n), out_shape=jax.Shape...  53.6 us
    unnamed x1, local copies, waits for them, and re-layouts  1.32 us

profile of v1, /device:TPU:0, one launch (start us, length us, event | category | flops | bytes accessed | tf_op | source)
XLA Modules:
  0.0 54.9 jit_solution(9615162939934529148)
XLA Ops:
  0.0 53.6 %shard_map.145 = bf16[32,256]{1,0:T(8,128)(2,1)} custom-call(s32[32]{0:T(128)} %lengths.1, bf16[32,256]{1,0:T(8,128)(2,1)} %stream.1, bf16[256]{0:T(256)(128)(2,1)} %gain_in.1, bf16[1024]{0:T(1024)(128)(2,1)} %gain_att.1, bf16[256]{0:T(256)(128)(2,1)} %gain_mlp.1, f32[32,8,128]{2,1,0:T(8,128)} %decay.1, bf16[16,4096]{1,0:T(8,128)(2,1)} %bitcast.1, ...), custom_call_target="tpu_custom_call" | custom-call | tf_op jit(solution)/shard_map/pallas_call | solution.py:596
  53.6 1.3 %copy.17 = bf16[32,256]{1,0:T(8,128)(2,1)} copy(bf16[32,256]{1,0:T(8,128)(2,1)} %shard_map.145) | data formatting | bytes 32768

commit v2 on v1

--- a/solution.py
+++ b/solution.py
@@ -152,7 +152,9 @@
     )
 
 
-Q, STAT, KV, Q_ALL, OUT, PEAK, ATT, SQUARE, MIX, UP, RELAY, HID, HID_RELAY, PAIR = range(14)
+Q, STAT, KV, Q_ALL, OUT, PEAK, ATT, SQUARE, MIX, GAIN, SWAP_ONE, SWAP_TWO = range(12)
+TO_RELAY, STRAIGHT, FROM_RELAY, HID_STRAIGHT, HID_LEVEL, HID_ON = 12, 13, 14, 15, 17, 21
+SENDS, ARRIVALS = 22, 29
 
 
 def layer_kernel(
@@ -161,7 +163,7 @@
     w_forget, w_query, w_key, w_value, keys, values, w_out, w_up, w_down,
     out,
     len_s, x_v, gi_v, ga_v, gm_v, decay_v,
-    wf_v, wq_v, wk_v, wv_v, keys_v, values_v, wo_v, wu_v, wd_v,
+    wf_v, wq_v, wk_v, wv_v, keys_v, keys_turned, values_v, wo_v, wu_v, wd_v,
     gain_far, q_send, q_recv, st_send, st_recv, kv_send, kv_recv,
     q_own, q_all, q_float, o_float, o_send, o_recv, pk_send, pk_recv,
     att_own, att_all, sq_own, sq_all, send5, recv5,
@@ -182,6 +184,7 @@
     chunks = cache_sem.shape[1]
     per_chunk = seqs // chunks
     width_all = cols * kv_n
+    others = kv_n - 1
     score_scale = 1.0 / math.sqrt(dim)
     together = math.gcd(8, per_chunk)
 
@@ -230,35 +233,23 @@
         part = pl.ds(chunk * per_chunk, per_chunk)
         return pltpu.make_async_copy(src.at[part], dst.at[part], cache_sem.at[which, chunk])
 
-    def remote(phase, slot, src, dst, device, core):
+    def remote(sent, landed, src, dst, device, core):
         return pltpu.make_async_remote_copy(
-            src_ref=src, dst_ref=dst,
-            send_sem=ssem.at[phase, slot], recv_sem=rsem.at[phase, slot],
+            src_ref=src, dst_ref=dst, send_sem=ssem.at[sent], recv_sem=rsem.at[landed],
             device_id=(device, core), device_id_type=pl.DeviceIdType.MESH,
         )
 
-    started = []
-
-    def go(copy):
-        copy.start()
-        started.append(copy)
-
-    def drain():
-        for copy in started:
-            copy.wait_send()
-        started.clear()
+    def all_of(index, held):
+        return remote(index, index, held, held, me, far)
 
     def scatter(phase, send, recv, k):
-        return remote(phase, k, send.at[peers[k]], recv.at[k], peers[k], far)
+        remote(phase, phase, send.at[peers[k]], recv.at[k], peers[k], far).start()
 
     def row_to(phase, src, recv, k):
-        return remote(phase, k, src, recv.at[pl.ds(k, 1)], peers[k], far)
+        remote(phase, phase, src, recv.at[pl.ds(k, 1)], peers[k], far).start()
 
     def spread(phase, own, held, k):
-        return remote(phase, k, own, held.at[me], peers[k], far)
-
-    def landed(phase, own, held, k):
-        return remote(phase, k, own, held.at[peers[k]], peers[k], far)
+        remote(phase, phase, own, held.at[me], peers[k], far).start()
 
     for copy in first_loads[:4]:
         copy.wait()
@@ -291,25 +282,41 @@
         copy.wait()
     for chunk in range(chunks):
         cache_copy(0, chunk).start()
+    for chunk in range(chunks):
         cache_copy(1, chunk).start()
     for copy in late_loads:
         copy.start()
     pl.semaphore_wait(barrier, kv_n)
     for k in far_first:
-        go(scatter(Q, q_send, q_recv, k))
-        go(row_to(STAT, st_send.at[pl.ds(peers[k] % heads, 1)], st_recv, k))
-    gain_swap = remote(PAIR, 0, ga_v, gain_far, me, far)
-    go(gain_swap)
+        scatter(Q, q_send, q_recv, k)
+        row_to(STAT, st_send.at[pl.ds(peers[k] % heads, 1)], st_recv, k)
+    gain_swap = remote(GAIN, GAIN, ga_v, gain_far, me, far)
+    gain_swap.start()
     for place, weight in enumerate((wk_v, wv_v)):
         by_owner(
             kv_send, jnp.dot(scaled, weight[...], preferred_element_type=f32).astype(bf16), place
         )
     for k in far_first:
-        go(scatter(KV, kv_send, kv_recv, k))
+        scatter(KV, kv_send, kv_recv, k)
     total = jnp.zeros((rows, dim), f32)
+
+    def turn_chunk(chunk, carry):
+        cache_copy(0, chunk).wait()
+
+        def turn(i, c):
+            s = chunk * per_chunk + i
+            for h in range(heads):
+                keys_turned[
+                    s, h % 2 * dim:(h % 2 + 1) * dim, h // 2 * pos_here:(h // 2 + 1) * pos_here
+                ] = keys_v[s, h].T
+            return c
+
+        return lax.fori_loop(0, per_chunk, turn, carry)
+
+    lax.fori_loop(0, chunks // 2, turn_chunk, 0)
+    all_of(STAT, st_recv).wait_recv()
+    all_of(Q, q_recv).wait_recv()
     for k in range(kv_n):
-        row_to(STAT, st_send.at[pl.ds(0, 1)], st_recv, k).wait_recv()
-        scatter(Q, q_send, q_recv, k).wait_recv()
         total = total + q_recv[k].astype(f32)
     stat_row = jnp.sum(st_recv[...], axis=0, keepdims=True)
     first_lane = my_group * rows
@@ -319,36 +326,49 @@
     query = (total * scale_in).astype(bf16)
     q_own[...] = query
     for k in far_first:
-        go(spread(Q_ALL, q_own, q_all, k))
+        spread(Q_ALL, q_own, q_all, k)
     gate = to_column(stat_row, rows, first_lane + 32) * scale_in
     forget = jnp.minimum(gate, 0.0) - jnp.log1p(jnp.exp(-jnp.abs(gate)))
 
-    for k in range(kv_n):
-        landed(Q_ALL, q_own, q_all, k).wait_recv()
+    lax.fori_loop(chunks // 2, chunks, turn_chunk, 0)
+    all_of(Q_ALL, q_all).wait_recv()
     q_float[...] = q_all[...].reshape(kv_n * rows, dim).astype(f32)
     head_row = rows_of((heads, pos_here))
     position = me * pos_here + lanes_of((heads, pos_here))
     lane_h = lanes_of((heads, LANES))
+
+    even = rows_of((heads, dim)) % 2 == 0
+
+    def in_pairs(cache, s):
+        return jnp.concatenate(
+            [
+                jnp.concatenate([cache[s, h], cache[s, h + 1]], axis=1)
+                for h in range(0, heads, 2)
+            ],
+            axis=0,
+        )
 
     def some_sequences(first_seq, marks):
         batch = [first_seq + i for i in range(together)]
         places = [
             pl.ds((s // rows) * (heads * rows) + s % rows, heads, stride=rows) for s in batch
         ]
-        q_parts = [q_float[mine, :].astype(bf16) for mine in places]
+        q_parts = [q_float[mine, :] for mine in places]
         everies = [
             lax.dot_general(
-                q_s, keys_v[s].reshape(heads * pos_here, dim), last,
-                preferred_element_type=f32,
+                jnp.concatenate(
+                    [jnp.where(even, q_s, 0.0), jnp.where(even, 0.0, q_s)], axis=1
+                ).astype(bf16),
+                keys_turned[s], (((1,), (0,)), ((), ())), preferred_element_type=f32,
             )
             for q_s, s in zip(q_parts, batch)
         ]
         spreads = []
         for every, s in zip(everies, batch):
             score = every[:, :pos_here]
-            for h in range(1, heads):
+            for pair in range(1, heads // 2):
                 score = jnp.where(
-                    head_row == h, every[:, h * pos_here:(h + 1) * pos_here], score
+                    head_row // 2 == pair, every[:, pair * pos_here:(pair + 1) * pos_here], score
                 )
             score = score * score_scale + decay_v[s]
             live = position < len_s[s]
@@ -357,22 +377,20 @@
             probs = jnp.where(live, jnp.exp(score - peak), 0.0)
             block_total = jnp.sum(probs, axis=1, keepdims=True)
             spreads.append(jnp.concatenate(
-                [jnp.where(head_row == h, probs, 0.0) for h in range(heads)], axis=1
+                [jnp.where(head_row // 2 == pair, probs, 0.0) for pair in range(heads // 2)],
+                axis=1,
             ).astype(bf16))
             marks = jnp.where(lane_h == s % rows, peak, marks)
             marks = jnp.where(lane_h == s % rows + rows, block_total, marks)
         outs = [
-            jnp.dot(
-                part, values_v[s].reshape(heads * pos_here, dim), preferred_element_type=f32
-            )
+            jnp.dot(part, in_pairs(values_v, s), preferred_element_type=f32)
             for part, s in zip(spreads, batch)
         ]
         for mine, out_s in zip(places, outs):
-            o_float[mine, :] = out_s
+            o_float[mine, :] = jnp.where(even, out_s[:, :dim], out_s[:, dim:])
         return marks
 
     def one_chunk(chunk, marks):
-        cache_copy(0, chunk).wait()
         cache_copy(1, chunk).wait()
 
         def inner(i, c):
@@ -388,12 +406,12 @@
         pk_send[g * heads:(g + 1) * heads, :] = marks
     o_send[...] = o_float[...].astype(bf16).reshape(kv_n, rows, dim)
     for k in far_first:
-        go(scatter(OUT, o_send, o_recv, k))
-        go(row_to(PEAK, pk_send.at[pl.ds(peers[k], 1)], pk_recv, k))
+        scatter(OUT, o_send, o_recv, k)
+        row_to(PEAK, pk_send.at[pl.ds(peers[k], 1)], pk_recv, k)
 
     keys_total = jnp.zeros((2 * rows, dim), f32)
+    all_of(KV, kv_recv).wait_recv()
     for k in range(kv_n):
-        scatter(KV, kv_send, kv_recv, k).wait_recv()
         keys_total = keys_total + kv_recv[k].astype(f32)
     key_new = (keys_total[:rows] * scale_in).astype(bf16).astype(f32)
     value_new = (keys_total[rows:] * scale_in).astype(bf16).astype(f32)
@@ -404,8 +422,12 @@
     for h in range(1, heads):
         gain_head = jnp.where(my_head == h, gain_here[:, h * dim:(h + 1) * dim], gain_head)
 
-    for k in range(kv_n):
-        row_to(PEAK, pk_send.at[pl.ds(0, 1)], pk_recv, k).wait_recv()
+    for copy in late_loads:
+        copy.wait()
+    for index, held in ((Q, q_recv), (STAT, st_recv), (KV, kv_recv), (Q_ALL, q_all)):
+        all_of(index, held).wait_send()
+    gain_swap.wait_send()
+    all_of(PEAK, pk_recv).wait_recv()
     peaks = pk_recv[...]
     top_row = jnp.max(peaks, axis=0, keepdims=True)
     shares = jnp.exp(peaks - top_row)
@@ -417,8 +439,8 @@
     past_weight = jnp.exp(peak_all - top)
     own_weight = jnp.exp(own_score - top)
     out_all = jnp.zeros((rows, dim), f32)
+    all_of(OUT, o_recv).wait_recv()
     for k in range(kv_n):
-        scatter(OUT, o_send, o_recv, k).wait_recv()
         out_all = out_all + share_columns[k] * o_recv[k].astype(f32)
     attended_one = (out_all * past_weight + value_new * own_weight) / (
         total_all * past_weight + own_weight
@@ -427,18 +449,11 @@
     squares_one = jnp.sum(attended_one * attended_one, axis=1, keepdims=True)
     sq_own[...] = jnp.broadcast_to(to_row(squares_one, first_lane), sq_own.shape)
     for k in far_first:
-        go(spread(ATT, att_own, att_all, k))
-        go(row_to(SQUARE, sq_own.at[pl.ds(0, 1)], sq_all, k))
-
-    for copy in late_loads:
-        copy.wait()
-    drain_before = list(started[:-2 * kv_n])
-    for copy in drain_before:
-        copy.wait_send()
-    del started[:len(drain_before)]
-    for k in range(kv_n):
-        landed(ATT, att_own, att_all, k).wait_recv()
-        row_to(SQUARE, sq_own.at[pl.ds(0, 1)], sq_all, k).wait_recv()
+        spread(ATT, att_own, att_all, k)
+        row_to(SQUARE, sq_own.at[pl.ds(0, 1)], sq_all, k)
+
+    all_of(ATT, att_all).wait_recv()
+    all_of(SQUARE, sq_all).wait_recv()
     attended_in = jnp.concatenate(
         [
             jnp.concatenate([att_all[g * heads + h] for g in range(groups)], axis=0)
@@ -450,8 +465,8 @@
     att_squares = to_column(jnp.sum(sq_all[...], axis=0, keepdims=True), seqs, 0)
     send5[:, :cols] = part_out
     send5[:, cols:] = jnp.broadcast_to(att_squares, (seqs, LANES))
-    swap5 = remote(PAIR, 1, send5, recv5, me, far)
-    go(swap5)
+    swap5 = remote(SWAP_ONE, SWAP_ONE, send5, recv5, me, far)
+    swap5.start()
     swap5.wait_recv()
     width_att = attended_in.shape[1] * 2
     scale_att = lax.rsqrt((att_squares + recv5[:, cols:cols + 1]) / width_att + norm_eps)
@@ -461,102 +476,132 @@
     mixer_in = (residual * gm_v[...].astype(f32).reshape(1, -1)).astype(bf16)
     mixer_squares = jnp.sum(residual * residual, axis=1, keepdims=True)
 
-    def up(owner):
-        columns = pl.ds(pl.multiple_of(owner * hidden_here, LANES), hidden_here)
+    def up(apart):
+        width = PLANE * hidden_here
+        columns = pl.ds(pl.multiple_of(levels[apart] * width, LANES), width)
         return jnp.dot(mixer_in, wu_v[:, columns], preferred_element_type=f32)
 
-    def to_relay(k):
+    def store_up(apart):
+        part = up(apart).astype(bf16)
+        for place in range(PLANE):
+            up_send[apart * PLANE + place] = part[
+                :, place * hidden_here:(place + 1) * hidden_here
+            ]
+
+    def to_relay(p):
         return remote(
-            UP, k, up_send.at[k], relay_recv.at[k - 2 * PLANE], peers[k % PLANE], far
-        )
-
-    def from_relay(apart):
-        index = apart - 2
+            TO_RELAY, TO_RELAY, up_send.at[2 * PLANE + spots[p]], relay_recv.at[p], peers[p], far
+        )
+
+    from_relay = remote(
+        FROM_RELAY, FROM_RELAY, relay_send, up_recv.at[others - PLANE], peers[2 * PLANE], far
+    )
+
+    def straight(k):
+        apart, p = k // PLANE, k % PLANE
+        slot = k - 1 if k < 2 * PLANE else k - 1 - PLANE
         return remote(
-            RELAY, index, relay_send.at[index], up_recv.at[index], peers[apart * PLANE], far
-        )
-
-    def straight(k):
-        return remote(UP, k, up_send.at[k], up_recv.at[k + 1], peers[k], tp)
-
-    for apart in (3, 2):
-        for p in plane_order:
-            k = apart * PLANE + p
-            up_send[k] = up(peers[k]).astype(bf16)
-            go(to_relay(k))
+            STRAIGHT, STRAIGHT, up_send.at[apart * PLANE + spots[p]], up_recv.at[slot],
+            peers[k], tp,
+        )
+
+    store_up(2)
+    for p in plane_order:
+        to_relay(p).start()
+    store_up(3)
+    for p in plane_order:
+        straight(3 * PLANE + p).start()
     mix_own[...] = jnp.broadcast_to(to_row(mixer_squares, 0), mix_own.shape)
     for k in far_first:
-        go(row_to(MIX, mix_own.at[pl.ds(0, 1)], mix_all, k))
-    for apart in (1, 0):
-        for p in plane_order:
-            k = apart * PLANE + p
-            if k:
-                up_send[k] = up(peers[k]).astype(bf16)
-                go(straight(k))
-    pre_act = up(me)
-    for apart in (3, 2):
-        relayed = None
-        for p in (0, 1, 2, 3):
-            k = apart * PLANE + p
-            to_relay(k).wait_recv()
-            block = relay_recv[k - 2 * PLANE].astype(f32)
-            relayed = block if relayed is None else relayed + block
-        relay_send[apart - 2] = relayed.astype(bf16)
-        go(from_relay(apart))
-    for k in range(kv_n):
-        row_to(MIX, mix_own.at[pl.ds(0, 1)], mix_all, k).wait_recv()
+        row_to(MIX, mix_own.at[pl.ds(0, 1)], mix_all, k)
+    store_up(1)
+    for p in plane_order:
+        straight(PLANE + p).start()
+    store_up(0)
+    for p in plane_order[:-1]:
+        straight(p).start()
+    pre_act = up_send[spot].astype(f32)
+    all_of(TO_RELAY, relay_recv).wait_recv()
+    relayed = relay_recv[0].astype(f32)
+    for p in range(1, PLANE):
+        relayed = relayed + relay_recv[p].astype(f32)
+    relay_send[...] = relayed.astype(bf16)
+    from_relay.start()
+    for index, held in ((OUT, o_recv), (PEAK, pk_recv), (ATT, att_all), (SQUARE, sq_all)):
+        all_of(index, held).wait_send()
+    swap5.wait_send()
+    all_of(MIX, mix_all).wait_recv()
     mixer_total = to_column(jnp.sum(mix_all[...], axis=0, keepdims=True), seqs, 0)
     scale_mixer = lax.rsqrt(mixer_total / width_all + norm_eps)
-    for k in range(1, 2 * PLANE):
-        straight(k).wait_recv()
-        pre_act = pre_act + up_recv[k + 1].astype(f32)
-    for apart in (2, 3):
-        from_relay(apart).wait_recv()
-        pre_act = pre_act + up_recv[apart - 2].astype(f32)
+    all_of(STRAIGHT, up_recv.at[pl.ds(0, others - PLANE)]).wait_recv()
+    for slot in range(others - PLANE):
+        pre_act = pre_act + up_recv[slot].astype(f32)
+    from_relay.wait_recv()
+    pre_act = pre_act + up_recv[others - PLANE].astype(f32)
     hidden = jnp.maximum(pre_act * scale_mixer, 0.0)
     hid_all[me] = (hidden * hidden).astype(bf16)
 
-    def to_level(apart):
+    half = seqs // 2
+
+    def to_level(apart, part):
+        some = pl.ds(part * half, half)
         return remote(
-            HID_RELAY, apart - 2, hid_all.at[me], hid_relay.at[apart - 2],
-            peers[apart * PLANE], far,
-        )
-
-    def onward(apart, p):
+            HID_LEVEL, HID_LEVEL + 2 * (apart - 2) + part, hid_all.at[me, some],
+            hid_relay.at[apart - 2, some], peers[apart * PLANE], far,
+        )
+
+    def onward(apart, part, p):
+        some = pl.ds(part * half, half)
         return remote(
-            HID, apart * PLANE + p, hid_relay.at[apart - 2],
-            hid_all.at[peers[apart * PLANE]], peers[p], far,
+            HID_ON, HID_ON + (apart - 2) * PLANE + p, hid_relay.at[apart - 2, some],
+            hid_all.at[peers[apart * PLANE], some], peers[p], far,
         )
 
     def arrived(k):
-        return remote(HID, k, hid_all.at[me], hid_all.at[peers[k]], peers[k], tp)
-
-    for apart in (3, 2):
-        go(to_level(apart))
+        index = HID_ON + k - 2 * PLANE
+        return remote(index, index, hid_all.at[me], hid_all.at[peers[k]], peers[k], tp)
+
+    for part in (0, 1):
+        for apart in (2, 3):
+            to_level(apart, part).start()
     for apart in (0, 1):
         for p in plane_order:
             k = apart * PLANE + p
             if k:
-                go(remote(HID, k, hid_all.at[me], hid_all.at[me], peers[k], tp))
+                remote(
+                    HID_STRAIGHT, HID_STRAIGHT + apart, hid_all.at[me], hid_all.at[me],
+                    peers[k], tp,
+                ).start()
 
     def down(owner):
         depth = pl.ds(pl.multiple_of(owner * hidden_here, LANES), hidden_here)
         return jnp.dot(hid_all[owner], wd_v[depth, :], preferred_element_type=f32)
 
     part_down = down(me)
-    for apart in (2, 3):
-        to_level(apart).wait_recv()
-        for p in plane_order:
-            go(onward(apart, p))
-    for k in range(1, kv_n):
+    for part in (0, 1):
+        for apart in (2, 3):
+            to_level(apart, part).wait_recv()
+            for p in plane_order:
+                onward(apart, part, p).start()
+    blocks = up_send.at[pl.ds(0, PLANE - 1)], up_send.at[pl.ds(0, PLANE)]
+    for apart in (0, 1):
+        all_of(HID_STRAIGHT + apart, blocks[apart]).wait_recv()
+        for p in range(PLANE):
+            if apart + p:
+                part_down = part_down + down(peers[apart * PLANE + p])
+    all_of(MIX, mix_all).wait_send()
+    all_of(TO_RELAY, relay_recv).wait_send()
+    all_of(STRAIGHT, up_recv.at[pl.ds(0, others - PLANE)]).wait_send()
+    from_relay.wait_send()
+    all_of(HID_LEVEL, hid_relay).wait_send()
+    all_of(HID_STRAIGHT, up_send.at[pl.ds(0, 2 * PLANE - 1)]).wait_send()
+    for k in (8, 9, 10, 11, 12, 13, 14, 15):
         arrived(k).wait_recv()
         part_down = part_down + down(peers[k])
     send8[...] = part_down
-    swap8 = remote(PAIR, 2, send8, recv8, me, far)
-    go(swap8)
-    drain_before = list(started[:-1])
-    for copy in drain_before:
-        copy.wait_send()
+    swap8 = remote(SWAP_TWO, SWAP_TWO, send8, recv8, me, far)
+    swap8.start()
+    all_of(HID_ON, up_send.at[pl.ds(0, 2 * PLANE)]).wait_send()
     swap8.wait_recv()
     out[...] = (residual + (part_down + recv8[...])).astype(bf16)
     swap8.wait_send()
@@ -595,7 +640,7 @@
 
     return pl.pallas_call(
         functools.partial(layer_kernel, kv_n),
-        out_shape=jax.ShapeDtypeStruct((seqs, cols), bf16),
+        out_shape=pltpu.VMEM((seqs, cols), bf16),
         in_specs=[anywhere] * 15,
         out_specs=pl.BlockSpec(memory_space=pltpu.VMEM),
         scratch_shapes=[
@@ -610,6 +655,7 @@
             held(*w_key.shape),
             held(*w_value.shape),
             held(*keys_cache.shape),
+            held(seqs, 2 * dim, heads // 2 * pos_here),
             held(*values_cache.shape),
             held(*w_out.shape),
             held(*w_up.shape),
@@ -638,17 +684,17 @@
             held(8, LANES, kind=f32),
             held(kv_n, LANES, kind=f32),
             held(kv_n, seqs, hidden_here),
-            held(2 * PLANE, seqs, hidden_here),
-            held(2, seqs, hidden_here),
-            held(2 * PLANE + 1, seqs, hidden_here),
+            held(PLANE, seqs, hidden_here),
+            held(seqs, hidden_here),
+            held(kv_n - PLANE, seqs, hidden_here),
             held(2, seqs, hidden_here),
             held(kv_n, seqs, hidden_here),
             held(seqs, cols, kind=f32),
             held(seqs, cols, kind=f32),
             pltpu.SemaphoreType.DMA((13,)),
             pltpu.SemaphoreType.DMA((2, chunks)),
-            pltpu.SemaphoreType.DMA((14, kv_n)),
-            pltpu.SemaphoreType.DMA((14, kv_n)),
+            pltpu.SemaphoreType.DMA((SENDS,)),
+            pltpu.SemaphoreType.DMA((ARRIVALS,)),
         ],
         compiler_params=pltpu.CompilerParams(
             collective_id=0, has_side_effects=True, vmem_limit_bytes=60 * 1024 * 1024

time: 55.2 us -> 49.4 us (0.89)
  Pallas kernels: 53.6 us -> 48.5 us
  local copies, waits for them, and re-layouts: 1.32 us -> 0.61 us
    pallas_call x1, Pallas kernels: 53.6 us -> 48.5 us  [layer(): pl.pallas_call(functools.partial(layer_kernel, kv_n), out_shape=pltpu.VME...]
    unnamed x1, local copies, waits for them, and re-layouts: 1.32 us -> 0.61 us
where the time goes in v2:
time: 49.4 us; the launch traced here: 49.1 us
  Pallas kernels  48.5 us (98%)
  local copies, waits for them, and re-layouts  0.61 us (1%)
    pallas_call x1, Pallas kernels, layer(): pl.pallas_call(functools.partial(layer_kernel, kv_n), out_shape=pltpu.VME...  48.5 us

profile of v2, /device:TPU:0, one launch (start us, length us, event | category | flops | bytes accessed | tf_op | source)
XLA Modules:
  0.0 49.1 jit_solution(1974375615708692559)
XLA Ops:
  0.0 48.5 %shard_map.145 = bf16[32,256]{1,0:T(8,128)(2,1)S(1)} custom-call(s32[32]{0:T(128)} %lengths.1, bf16[32,256]{1,0:T(8,128)(2,1)} %stream.1, bf16[256]{0:T(256)(128)(2,1)} %gain_in.1, bf16[1024]{0:T(1024)(128)(2,1)} %gain_att.1, bf16[256]{0:T(256)(128)(2,1)} %gain_mlp.1, f32[32,8,128]{2,1,0:T(8,128)} %decay.1, bf16[16,4096]{1,0:T(8,128)(2,1)} %bitcast.1, ...), custom_call_target="tpu_custom_call" | custom-call | tf_op jit(solution)/shard_map/pallas_call | solution.py:641
  48.5 0.6 %copy.17 = bf16[32,256]{1,0:T(8,128)(2,1)} copy(bf16[32,256]{1,0:T(8,128)(2,1)S(1)} %shard_map.145) | data formatting | bytes 32768

commit v3 on v2

--- a/solution.py
+++ b/solution.py
@@ -154,7 +154,7 @@
 
 Q, STAT, KV, Q_ALL, OUT, PEAK, ATT, SQUARE, MIX, GAIN, SWAP_ONE, SWAP_TWO = range(12)
 TO_RELAY, STRAIGHT, FROM_RELAY, HID_STRAIGHT, HID_LEVEL, HID_ON = 12, 13, 14, 15, 17, 21
-SENDS, ARRIVALS = 22, 29
+SENDS, ARRIVALS, STRAIGHT_OWN = 22, 30, 29
 
 
 def layer_kernel(
@@ -168,7 +168,7 @@
     q_own, q_all, q_float, o_float, o_send, o_recv, pk_send, pk_recv,
     att_own, att_all, sq_own, sq_all, send5, recv5,
     mix_own, mix_all, up_send, relay_recv, relay_send, up_recv,
-    hid_relay, hid_all, send8, recv8,
+    hid_all, send8, recv8,
     load_sem, cache_sem, ssem, rsem,
 ):
     me = lax.axis_index("kv")
@@ -296,8 +296,6 @@
         by_owner(
             kv_send, jnp.dot(scaled, weight[...], preferred_element_type=f32).astype(bf16), place
         )
-    for k in far_first:
-        scatter(KV, kv_send, kv_recv, k)
     total = jnp.zeros((rows, dim), f32)
 
     def turn_chunk(chunk, carry):
@@ -327,6 +325,8 @@
     q_own[...] = query
     for k in far_first:
         spread(Q_ALL, q_own, q_all, k)
+    for k in far_first:
+        scatter(KV, kv_send, kv_recv, k)
     gate = to_column(stat_row, rows, first_lane + 32) * scale_in
     forget = jnp.minimum(gate, 0.0) - jnp.log1p(jnp.exp(-jnp.abs(gate)))
 
@@ -403,11 +403,18 @@
         marks = lax.fori_loop(
             g * group_chunks, (g + 1) * group_chunks, one_chunk, jnp.zeros((heads, LANES), f32)
         )
-        pk_send[g * heads:(g + 1) * heads, :] = marks
-    o_send[...] = o_float[...].astype(bf16).reshape(kv_n, rows, dim)
-    for k in far_first:
-        scatter(OUT, o_send, o_recv, k)
-        row_to(PEAK, pk_send.at[pl.ds(peers[k], 1)], pk_recv, k)
+        mine = slice(g * heads, (g + 1) * heads)
+        pk_send[mine, :] = marks
+        o_send[mine] = o_float[g * heads * rows:(g + 1) * heads * rows, :].astype(bf16).reshape(
+            heads, rows, dim
+        )
+        for step in (1, 0):
+            for p in plane_order:
+                owner = (g * 2 + (level + step) % 2) * PLANE + spots[p]
+                remote(OUT, OUT, o_send.at[owner], o_recv.at[me], owner, far).start()
+                remote(
+                    PEAK, PEAK, pk_send.at[pl.ds(owner, 1)], pk_recv.at[pl.ds(me, 1)], owner, far
+                ).start()
 
     keys_total = jnp.zeros((2 * rows, dim), f32)
     all_of(KV, kv_recv).wait_recv()
@@ -501,7 +508,8 @@
         apart, p = k // PLANE, k % PLANE
         slot = k - 1 if k < 2 * PLANE else k - 1 - PLANE
         return remote(
-            STRAIGHT, STRAIGHT, up_send.at[apart * PLANE + spots[p]], up_recv.at[slot],
+            STRAIGHT, STRAIGHT_OWN if k < PLANE else STRAIGHT,
+            up_send.at[apart * PLANE + spots[p]], up_recv.at[slot],
             peers[k], tp,
         )
 
@@ -533,11 +541,16 @@
     all_of(MIX, mix_all).wait_recv()
     mixer_total = to_column(jnp.sum(mix_all[...], axis=0, keepdims=True), seqs, 0)
     scale_mixer = lax.rsqrt(mixer_total / width_all + norm_eps)
-    all_of(STRAIGHT, up_recv.at[pl.ds(0, others - PLANE)]).wait_recv()
-    for slot in range(others - PLANE):
+    remote(
+        STRAIGHT, STRAIGHT, up_send.at[pl.ds(0, 2 * PLANE)], up_send.at[pl.ds(0, 2 * PLANE)], me, far
+    ).wait_recv()
+    for slot in range(PLANE - 1, others - PLANE):
         pre_act = pre_act + up_recv[slot].astype(f32)
     from_relay.wait_recv()
     pre_act = pre_act + up_recv[others - PLANE].astype(f32)
+    all_of(STRAIGHT_OWN, up_send.at[pl.ds(0, PLANE - 1)]).wait_recv()
+    for slot in range(PLANE - 1):
+        pre_act = pre_act + up_recv[slot].astype(f32)
     hidden = jnp.maximum(pre_act * scale_mixer, 0.0)
     hid_all[me] = (hidden * hidden).astype(bf16)
 
@@ -547,14 +560,14 @@
         some = pl.ds(part * half, half)
         return remote(
             HID_LEVEL, HID_LEVEL + 2 * (apart - 2) + part, hid_all.at[me, some],
-            hid_relay.at[apart - 2, some], peers[apart * PLANE], far,
+            hid_all.at[me, some], peers[apart * PLANE], tp,
         )
 
     def onward(apart, part, p):
         some = pl.ds(part * half, half)
         return remote(
-            HID_ON, HID_ON + (apart - 2) * PLANE + p, hid_relay.at[apart - 2, some],
-            hid_all.at[peers[apart * PLANE], some], peers[p], far,
+            HID_ON, HID_ON + (apart - 2) * PLANE + p, hid_all.at[peers[apart * PLANE], some],
+            hid_all.at[peers[apart * PLANE], some], peers[p], tp,
         )
 
     def arrived(k):
@@ -581,7 +594,7 @@
     for part in (0, 1):
         for apart in (2, 3):
             to_level(apart, part).wait_recv()
-            for p in plane_order:
+            for p in plane_order[:-1]:
                 onward(apart, part, p).start()
     blocks = up_send.at[pl.ds(0, PLANE - 1)], up_send.at[pl.ds(0, PLANE)]
     for apart in (0, 1):
@@ -593,15 +606,16 @@
     all_of(TO_RELAY, relay_recv).wait_send()
     all_of(STRAIGHT, up_recv.at[pl.ds(0, others - PLANE)]).wait_send()
     from_relay.wait_send()
-    all_of(HID_LEVEL, hid_relay).wait_send()
+    all_of(HID_LEVEL, up_send.at[pl.ds(0, 2)]).wait_send()
     all_of(HID_STRAIGHT, up_send.at[pl.ds(0, 2 * PLANE - 1)]).wait_send()
     for k in (8, 9, 10, 11, 12, 13, 14, 15):
-        arrived(k).wait_recv()
+        if k % PLANE:
+            arrived(k).wait_recv()
         part_down = part_down + down(peers[k])
     send8[...] = part_down
     swap8 = remote(SWAP_TWO, SWAP_TWO, send8, recv8, me, far)
     swap8.start()
-    all_of(HID_ON, up_send.at[pl.ds(0, 2 * PLANE)]).wait_send()
+    all_of(HID_ON, up_send.at[pl.ds(0, 2 * PLANE - 2)]).wait_send()
     swap8.wait_recv()
     out[...] = (residual + (part_down + recv8[...])).astype(bf16)
     swap8.wait_send()
@@ -687,7 +701,6 @@
             held(PLANE, seqs, hidden_here),
             held(seqs, hidden_here),
             held(kv_n - PLANE, seqs, hidden_here),
-            held(2, seqs, hidden_here),
             held(kv_n, seqs, hidden_here),
             held(seqs, cols, kind=f32),
             held(seqs, cols, kind=f32),

time: 49.4 us -> 48.7 us (0.986)
  Pallas kernels: 48.5 us -> 47.8 us
    pallas_call x1, Pallas kernels: 48.5 us -> 47.8 us  [layer(): pl.pallas_call(functools.partial(layer_kernel, kv_n), out_shape=pltpu.VME...]
where the time goes in v3:
time: 48.7 us; the launch traced here: 48.5 us
  Pallas kernels  47.8 us (98%)
  local copies, waits for them, and re-layouts  0.61 us (1%)
    pallas_call x1, Pallas kernels, layer(): pl.pallas_call(functools.partial(layer_kernel, kv_n), out_shape=pltpu.VME...  47.8 us

profile of v3, /device:TPU:0, one launch (start us, length us, event | category | flops | bytes accessed | tf_op | source)
XLA Modules:
  0.0 48.5 jit_solution(16339425787788970323)
XLA Ops:
  0.0 47.8 %shard_map.145 = bf16[32,256]{1,0:T(8,128)(2,1)S(1)} custom-call(s32[32]{0:T(128)} %lengths.1, bf16[32,256]{1,0:T(8,128)(2,1)} %stream.1, bf16[256]{0:T(256)(128)(2,1)} %gain_in.1, bf16[1024]{0:T(1024)(128)(2,1)} %gain_att.1, bf16[256]{0:T(256)(128)(2,1)} %gain_mlp.1, f32[32,8,128]{2,1,0:T(8,128)} %decay.1, bf16[16,4096]{1,0:T(8,128)(2,1)} %bitcast.1, ...), custom_call_target="tpu_custom_call" | custom-call | tf_op jit(solution)/shard_map/pallas_call | solution.py:655
  47.8 0.6 %copy.17 = bf16[32,256]{1,0:T(8,128)(2,1)} copy(bf16[32,256]{1,0:T(8,128)(2,1)S(1)} %shard_map.145) | data formatting | bytes 32768

commit v4 on v3

--- a/solution.py
+++ b/solution.py
@@ -646,7 +646,7 @@
         )
     rows = seqs * heads // kv_n
     hidden_here = units // kv_n
-    chunks = 4
+    chunks = 2
     anywhere = pl.BlockSpec(memory_space=pl.ANY)
 
     def held(*shape, kind=bf16):

time: 48.7 us -> 48.6 us (level)
  no operation moved by 1% of the time
where the time goes in v4:
time: 48.6 us; the launch traced here: 48.4 us
  Pallas kernels  47.8 us (98%)
  local copies, waits for them, and re-layouts  0.61 us (1%)
    pallas_call x1, Pallas kernels, layer(): pl.pallas_call(functools.partial(layer_kernel, kv_n), out_shape=pltpu.VME...  47.8 us

profile of v4, /device:TPU:0, one launch (start us, length us, event | category | flops | bytes accessed | tf_op | source)
XLA Modules:
  0.0 48.4 jit_solution(6279741510797611068)
XLA Ops:
  0.0 47.8 %shard_map.145 = bf16[32,256]{1,0:T(8,128)(2,1)S(1)} custom-call(s32[32]{0:T(128)} %lengths.1, bf16[32,256]{1,0:T(8,128)(2,1)} %stream.1, bf16[256]{0:T(256)(128)(2,1)} %gain_in.1, bf16[1024]{0:T(1024)(128)(2,1)} %gain_att.1, bf16[256]{0:T(256)(128)(2,1)} %gain_mlp.1, f32[32,8,128]{2,1,0:T(8,128)} %decay.1, bf16[16,4096]{1,0:T(8,128)(2,1)} %bitcast.1, ...), custom_call_target="tpu_custom_call" | custom-call | tf_op jit(solution)/shard_map/pallas_call | solution.py:655
  47.8 0.6 %copy.17 = bf16[32,256]{1,0:T(8,128)(2,1)} copy(bf16[32,256]{1,0:T(8,128)(2,1)S(1)} %shard_map.145) | data formatting | bytes 32768
